TPU v7x, 32 devices: a whole 2x2x4 slice. The times are simulated.
32 devices in a mesh: dp: 4 (over y, x), kv: 4 (over z), tp: 2 (over core).
Axes of the slice: x: 2, y: 2, z: 4, core: 2. Of those that a mesh axis runs over, the one named last changes fastest.
Arguments:
- tokens: bfloat16 [192, 2048], P(('dp', 'tp'), 'kv'), may hold values from -8 to 8
- mix_gain: float32 [2048], replicated, may hold values from 0.1 to 1.9
- w_gate: bfloat16 [2048, 4096], P(None, 'kv'), may hold values from -0.125 to 0.125
- w_value: bfloat16 [2048, 4096], P(None, 'kv'), may hold values from -0.125 to 0.125
- w_maps: bfloat16 [2048, 16384], P(None, 'kv'), may hold values from -0.125 to 0.125
- w_step: bfloat16 [2048, 64], replicated, may hold values from -0.125 to 0.125
- conv_value: float32 [4, 4096], P(None, 'kv'), may hold values from -0.5 to 0.5
- conv_maps: float32 [4, 16384], P(None, 'kv'), may hold values from -0.5 to 0.5
- past_value: bfloat16 [192, 3, 4096], P(('dp', 'tp'), None, 'kv'), may hold values from -6 to 6
- past_maps: bfloat16 [192, 3, 16384], P(('dp', 'tp'), None, 'kv'), may hold values from -6 to 6
- step_bias: float32 [64], P('kv'), may hold values from -3 to 0
- decay_log: float32 [64], P('kv'), may hold values from 0 to 2.77
- skip_gain: float32 [64], P('kv'), may hold values from 0.1 to 1.9
- head_gain: float32 [4096], P('kv'), may hold values from 0.1 to 1.9
- state: float32 [192, 64, 64, 128], P(('dp', 'tp'), 'kv'), may hold values from -2 to 2
- w_out: bfloat16 [4096, 2048], P('kv'), may hold values from -0.125 to 0.125
- mlp_gain: float32 [2048], replicated, may hold values from 0.1 to 1.9
- w_up: bfloat16 [2048, 8192], P(None, 'kv'), may hold values from -0.125 to 0.125
- w_down: bfloat16 [8192, 2048], P('kv'), may hold values from -0.09375 to 0.09375
Outputs:
- layer_out: bfloat16 [192, 2048], P(('dp', 'tp'), 'kv')
- state_next: float32 [192, 64, 64, 128], P(('dp', 'tp'), 'kv')
- value_tail: bfloat16 [192, 3, 4096], P(('dp', 'tp'), None, 'kv')
- maps_tail: bfloat16 [192, 3, 16384], P(('dp', 'tp'), None, 'kv')
All inputs are finite; a program needn't handle non-finite values.
Results may differ from a plain program's by a relative error of at most 0.0081.
Values may be sent and summed in bfloat16 or wider, within the bound.
A program may use at most 128 MiB of HBM per device.

v0:
```python
import jax
import jax.numpy as jnp
from jax import lax
from jax.sharding import PartitionSpec as P

HEAD_DIM = 64
STATE = 128


NORM_EPS = 1e-05


def rms_rows(matrix, gain_vec):
    widened = matrix.astype(jnp.float32)
    inv_scale = lax.rsqrt(jnp.mean(widened * widened, axis=-1, keepdims=True) + NORM_EPS)
    return (widened * inv_scale * gain_vec).astype(jnp.bfloat16)


def short_conv(past_rows, newest, kernel):
    window = jnp.concatenate([past_rows, newest[:, None, :]], axis=1)
    summed = jnp.sum(window.astype(jnp.float32) * kernel[None], axis=1)
    return (jax.nn.silu(summed), window[:, 1:, :])


def local(
    tokens,
    mix_gain,
    w_gate,
    w_value,
    w_maps,
    w_step,
    conv_value,
    conv_maps,
    past_value,
    past_maps,
    step_bias,
    decay_log,
    skip_gain,
    head_gain,
    state,
    w_out,
    mlp_gain,
    w_up,
    w_down,
):
    whole_rows = lax.all_gather(tokens, "kv", axis=1, tiled=True)
    batch_rows = whole_rows.shape[0]
    heads_here = state.shape[1]
    head_start = lax.axis_index("kv") * heads_here
    normed = rms_rows(whole_rows, mix_gain)
    gate_pre = jnp.dot(normed, w_gate, preferred_element_type=jnp.float32)
    step_cols = lax.dynamic_slice_in_dim(w_step, head_start, heads_here, 1)
    step_pre = jnp.dot(normed, step_cols, preferred_element_type=jnp.float32)
    value_new = jnp.dot(normed, w_value, preferred_element_type=jnp.float32).astype(jnp.bfloat16)
    maps_new = jnp.dot(normed, w_maps, preferred_element_type=jnp.float32).astype(jnp.bfloat16)
    value_act, value_tail = short_conv(past_value, value_new, conv_value)
    maps_act, maps_tail = short_conv(past_maps, maps_new, conv_maps)
    maps_act = lax.optimization_barrier(maps_act.astype(jnp.bfloat16))
    grouped = maps_act.astype(jnp.float32).reshape(batch_rows, -1, 2, STATE)
    per_group = heads_here // grouped.shape[1]
    in_map = jnp.repeat(grouped[:, :, 0], per_group, axis=1)
    out_map = jnp.repeat(grouped[:, :, 1], per_group, axis=1)
    head_values = value_act.reshape(batch_rows, heads_here, HEAD_DIM)
    step_size = jax.nn.softplus(step_pre + step_bias)
    decay_rate = jnp.exp(-step_size * jnp.exp(decay_log))
    written = (step_size[:, :, None] * head_values)[:, :, :, None] * in_map[:, :, None, :]
    state_next = decay_rate[:, :, None, None] * state + written
    read_out = (
        jnp.sum(state_next * out_map[:, :, None, :], axis=-1)
        + skip_gain[None, :, None] * head_values
    )
    gated_heads = read_out * jax.nn.silu(gate_pre.reshape(batch_rows, heads_here, HEAD_DIM))
    inv_scale = lax.rsqrt(jnp.mean(gated_heads * gated_heads, axis=-1, keepdims=True) + NORM_EPS)
    heads_out = gated_heads * inv_scale * head_gain.reshape(heads_here, HEAD_DIM)
    heads_out = heads_out.reshape(batch_rows, heads_here * HEAD_DIM).astype(jnp.bfloat16)
    partial_value = jnp.dot(heads_out, w_out, preferred_element_type=jnp.float32)
    own_part = lax.psum_scatter(partial_value, "kv", scatter_dimension=1, tiled=True)
    own_hidden = lax.optimization_barrier(
        (tokens.astype(jnp.float32) + own_part).astype(jnp.bfloat16)
    )
    hidden = lax.all_gather(own_hidden, "kv", axis=1, tiled=True)
    normed_mlp = rms_rows(hidden, mlp_gain)
    squared = jnp.square(jax.nn.relu(jnp.dot(normed_mlp, w_up, preferred_element_type=jnp.float32)))
    squared = squared.astype(jnp.bfloat16)
    partial_mlp = jnp.dot(squared, w_down, preferred_element_type=jnp.float32)
    mlp_part = lax.psum_scatter(partial_mlp, "kv", scatter_dimension=1, tiled=True)
    layer_out = (own_hidden.astype(jnp.float32) + mlp_part).astype(jnp.bfloat16)
    return (layer_out, state_next, value_tail, maps_tail)


def solution(mesh):
    in_specs = (
        P(("dp", "tp"), "kv"),
        P(),
        P(None, "kv"),
        P(None, "kv"),
        P(None, "kv"),
        P(),
        P(None, "kv"),
        P(None, "kv"),
        P(("dp", "tp"), None, "kv"),
        P(("dp", "tp"), None, "kv"),
        P("kv"),
        P("kv"),
        P("kv"),
        P("kv"),
        P(("dp", "tp"), "kv", None, None),
        P("kv", None),
        P(),
        P(None, "kv"),
        P("kv", None),
    )
    out_specs = (
        P(("dp", "tp"), "kv"),
        P(("dp", "tp"), "kv", None, None),
        P(("dp", "tp"), None, "kv"),
        P(("dp", "tp"), None, "kv"),
    )
    return jax.shard_map(local, mesh=mesh, in_specs=in_specs, out_specs=out_specs, check_vma=False)
```

profile of v0, /device:TPU:0, one launch (start us, length us, event | category | flops | bytes accessed | tf_op | source)
XLA Modules:
  0.0 126.5 jit_solution(10900179025579592787)
XLA Ops:
  7.2 0.0 copy-start
  7.2 0.0 reduce-scatter.3.cloned.1.call-start
  7.2 15.4 %all_gather.6 = bf16[24,2048]{1,0:T(8,128)(2,1)S(1)} all-gather(bf16[24,512]{1,0:T(8,128)(2,1)} %param.19), channel_id=1, replica_groups=mesh['dp'=4,'kv'=4,'tp'=2] {'kv'}, dimensions={1}, use_global_device_ids=true | all-gather | bytes 122880 | tf_op jit(solution)/shard_map/all_gather | solution.py:46
  22.6 0.1 fusion.6
  22.8 0.7 exp.34
  23.5 1.0 multiply_exponential_fusion
  24.4 0.1 copy.26
  24.5 2.9 %fusion.3 = bf16[24,1,1024]{2,0,1:T(8,128)(2,1)S(1)} fusion(bf16[2048,1024]{1,0:T(8,128)(2,1)} %param.22, bf16[24,2048]{1,0:T(8,128)(2,1)S(1)} %all_gather.6, f32[2048]{0:T(1024)} %param.20, f32[24]{0:T(128)S(1)} %add_rsqrt_fusion.2), kind=kOutput, calls=%fused_computation.9 | convolution fusion | flops 100884480 | bytes 4350048 | tf_op jit(solution)/shard_map/dot_general | solution.py:54
  27.4 1.0 multiply_reduce_fusion.2
  28.4 0.1 reduce_sum.60
  28.5 0.1 copy.25
  28.5 8.2 %fusion = bf16[24,1,4096]{2,0,1:T(8,128)(2,1)S(1)} fusion(bf16[2048,4096]{1,0:T(8,128)(2,1)} %param.23, bf16[24,2048]{1,0:T(8,128)(2,1)S(1)} %all_gather.6, f32[2048]{0:T(1024)} %param.20, f32[24]{0:T(128)S(1)} %add_rsqrt_fusion.2), kind=kOutput, calls=%fused_computation.3 | convolution fusion | flops 402948096 | bytes 17080416 | tf_op jit(solution)/shard_map/dot_general | solution.py:55
  36.7 0.0 copy-done.2
  36.7 0.0 copy-done.6
  36.8 0.2 multiply_reduce_fusion.1
  36.9 0.1 multiply_convert_fusion
  37.1 0.4 reshape.76
  37.5 0.3 fusion.35
  37.8 0.0 copy-done.4
  37.8 2.9 %fusion.30 = f32[24,1024]{1,0:T(8,128)S(1)} fusion(bf16[2048,1024]{1,0:T(8,128)(2,1)} %param.21, bf16[24,2048]{1,0:T(8,128)(2,1)S(1)} %all_gather.6, f32[2048]{0:T(1024)S(1)} %copy-done.4, f32[24]{0:T(128)S(1)} %add_rsqrt_fusion.2), kind=kOutput, calls=%fused_computation.54 | convolution fusion | flops 100859904 | bytes 4399200 | tf_op jit(solution)/shard_map/dot_general | solution.py:51
  40.7 0.1 reshape.74
  40.8 0.1 broadcast_multiply_fusion
  40.9 0.0 copy-start.9
  40.9 0.0 copy-start.8
  40.9 0.0 copy-start.3
  40.9 0.0 copy-start.5
  41.0 0.0 copy-start.7
  41.0 11.1 %multiply_reduce_fusion = (f32[24,16,64]{2,1,0:T(8,128)S(1)}, f32[24,16,64,128]{3,2,1,0:T(8,128)}) fusion(f32[24,16,128]{2,1,0:T(8,128)S(1)} %bitcast.13, f32[24,16,128]{2,1,0:T(8,128)S(1)} %bitcast.12, f32[24,16,64]{2,1,0:T(8,128)S(1)} %broadcast_multiply_fusion, f32[24,16,64,128]{3,2,1,0:T(8,128)} %param.33, f32[24,16]{1,0:T(8,128)S(1)} %copy.25), kind=kLoop, calls=%fused_computation | loop fusion | flops 15704064 | bytes 25757184 | tf_op jit(solution)/shard_map/reduce_sum | solution.py:69
  52.0 0.1 reduce_sum.63
  52.2 0.0 copy-done.9
  52.2 0.2 multiply_reduce_fusion.3
  52.4 0.1 mul.216
  52.5 0.1 mul.217
  52.6 0.1 mul.204
  52.7 0.1 mul.205
  52.8 3.5 %fusion.21 = f32[24,2048]{1,0:T(8,128)} fusion(bf16[1024,2048]{1,0:T(8,128)(2,1)} %param.34, f32[24,1024]{1,0:T(8,128)S(1)} %mul.217, f32[24,1024]{1,0:T(8,128)S(1)} %fusion.30, f32[24,1024]{1,0:T(8,128)S(1)} %reduce_sum.63, f32[24,1024]{1,0:T(8,128)S(1)} %multiply_reduce_fusion.2, f32[1024]{0:T(1024)S(1)} %copy-done.8, f32[1024]{0:T(1024)S(1)} %mul.205), kind=kOutput, calls=%fused_computation.40 | convolution fusion | flops 101007360 | bytes 4792320 | tf_op jit(solution)/shard_map/dot_general | solution.py:76
  56.3 0.0 reduce-scatter.3.cloned.1.call-update
  56.3 0.0 reduce-scatter.5.cloned.1.call-start
  56.4 0.7 fusion.12
  57.1 20.1 %reduce-scatter.3.cloned.1.call-done = f32[24,512]{1,0:T(8,128)} async-done(((f32[24,2048]{1,0:T(8,128)}), f32[24,512]{1,0:T(8,128)}) %reduce-scatter.3.cloned.1.call-update) | async-done | bytes 49168 | tf_op jit(solution)/shard_map/reduce_scatter | solution.py:77
  77.2 0.8 add_convert_fusion.1
  78.0 13.2 %all_gather.7 = bf16[24,2048]{1,0:T(8,128)(2,1)S(1)} all-gather(bf16[24,512]{1,0:T(8,128)(2,1)S(1)} %add_convert_fusion.1), channel_id=1, replica_groups=mesh['dp'=4,'kv'=4,'tp'=2] {'kv'}, dimensions={1}, use_global_device_ids=true | all-gather | bytes 122880 | tf_op jit(solution)/shard_map/all_gather | solution.py:81
  91.3 0.1 fusion.9
  91.4 8.8 %fusion.4 = f32[24,2048]{1,0:T(8,128)} fusion(bf16[2048,2048]{1,0:T(8,128)(2,1)} %param.37, bf16[2048,2048]{1,0:T(8,128)(2,1)} %param.36, bf16[24,2048]{1,0:T(8,128)(2,1)S(1)} %all_gather.7, f32[2048]{0:T(1024)S(1)} %copy-done.7, f32[24]{0:T(128)S(1)} %add_rsqrt_fusion.1), kind=kOutput, calls=%fused_computation.14 | convolution fusion | flops 402997248 | bytes 17080416 | tf_op jit(solution)/shard_map/dot_general | solution.py:85
  100.3 0.0 reduce-scatter.5.cloned.1.call-update
  100.3 0.9 fusion.5
  101.2 17.1 %reduce-scatter.5.cloned.1.call-done = f32[24,512]{1,0:T(8,128)} async-done(((f32[24,2048]{1,0:T(8,128)}), f32[24,512]{1,0:T(8,128)}) %reduce-scatter.5.cloned.1.call-update) | async-done | bytes 49168 | tf_op jit(solution)/shard_map/reduce_scatter | solution.py:86
  118.2 1.4 %add_convert_fusion = bf16[24,512]{1,0:T(8,128)(2,1)} fusion(f32[24,512]{1,0:T(8,128)} %reduce-scatter.5.cloned.1.call-done, bf16[24,512]{1,0:T(8,128)(2,1)S(1)} %add_convert_fusion.1), kind=kLoop, calls=%fused_computation.41 | loop fusion | flops 36864 | bytes 98304 | tf_op jit(solution)/shard_map/convert_element_type | solution.py:87
  (13 shorter events, 0.0 us)
Async XLA Ops:
  7.2 16.3 %copy-start = (bf16[2048,64]{0,1:T(8,128)(2,1)S(1)}, bf16[2048,64]{0,1:T(8,128)(2,1)}, u32[]{:S(2)}) copy-start(bf16[2048,64]{0,1:T(8,128)(2,1)} %param.24) | copy-start | bytes 786436
  7.2 70.0 %reduce-scatter.3.cloned.1.call-start = ((), (), s32[]{:S(2)}) async-start(), calls=%async_computation.2 | async-start | bytes 245760 | tf_op jit(solution)/shard_map/reduce_scatter | solution.py:77
  28.5 8.2 %copy-start.2 = (bf16[24,3,4096]{2,0,1:T(8,128)(2,1)S(1)}, bf16[24,3,4096]{2,0,1:T(8,128)(2,1)}, u32[]{:S(2)}) copy-start(bf16[24,3,4096]{2,0,1:T(8,128)(2,1)} %param.28) | copy-start | bytes 1769476
  28.5 8.2 %copy-start.6 = (f32[4,4096]{1,0:T(4,128)S(1)}, f32[4,4096]{1,0:T(4,128)}, u32[]{:S(2)}) copy-start(f32[4,4096]{1,0:T(4,128)} %param.26) | copy-start | bytes 196612
  28.5 9.2 %copy-start.4 = (f32[2048]{0:T(1024)S(1)}, f32[2048]{0:T(1024)}, u32[]{:S(2)}) copy-start(f32[2048]{0:T(1024)} %param.20) | copy-start | bytes 24580
  40.9 11.2 %copy-start.9 = (f32[16]{0:T(128)S(1)}, f32[16]{0:T(128)}, u32[]{:S(2)}) copy-start(f32[16]{0:T(128)} %param.31) | copy-start | bytes 196
  40.9 11.9 %copy-start.8 = (f32[1024]{0:T(1024)S(1)}, f32[1024]{0:T(1024)}, u32[]{:S(2)}) copy-start(f32[1024]{0:T(1024)} %param.32) | copy-start | bytes 12292
  40.9 15.5 %copy-start.3 = (bf16[24,3,1024]{2,0,1:T(8,128)(2,1)S(1)}, bf16[24,3,1024]{2,0,1:T(8,128)(2,1)}, u32[]{:S(2)}) copy-start(bf16[24,3,1024]{2,0,1:T(8,128)(2,1)} %param.27) | copy-start | bytes 442372
  40.9 36.3 %copy-start.5 = (bf16[24,512]{1,0:T(8,128)(2,1)S(1)}, bf16[24,512]{1,0:T(8,128)(2,1)}, u32[]{:S(2)}) copy-start(bf16[24,512]{1,0:T(8,128)(2,1)} %param.19) | copy-start | bytes 73732
  41.0 50.5 %copy-start.7 = (f32[2048]{0:T(1024)S(1)}, f32[2048]{0:T(1024)}, u32[]{:S(2)}) copy-start(f32[2048]{0:T(1024)} %param.35) | copy-start | bytes 24580
  56.3 61.9 %reduce-scatter.5.cloned.1.call-start = ((), (), s32[]{:S(2)}) async-start(), calls=%async_computation.3 | async-start | bytes 245760 | tf_op jit(solution)/shard_map/reduce_scatter | solution.py:86
  91.4 28.3 %copy-start.1 = (bf16[2048,64]{0,1:T(8,128)(2,1)S(1)}, bf16[2048,64]{0,1:T(8,128)(2,1)}, u32[]{:S(2)}) copy-start(bf16[2048,64]{0,1:T(8,128)(2,1)} %param.24) | copy-start | bytes 786436
Sparse Core Ops, SparseCore 0:
  56.5 20.7 reduce-scatter.2
  100.4 17.7 reduce-scatter.4
where the time goes:
time: 127 us
  waiting for transfers between devices  37.3 us (29%)
  blocking collectives  28.6 us (23%)
  matrix products  27.3 us (21%)
  other arithmetic  16.7 us (13%)
  between operations  14.2 us (11%)
  local copies, waits for them, and re-layouts  2.25 us (2%)
    reduce_scatter x1, waiting for transfers between devices, local(): lax.psum_scatter(partial_value, 'kv', scatter_dimension=1, tiled=True)  20.1 us
    reduce_scatter x1, waiting for transfers between devices, local(): lax.psum_scatter(partial_mlp, 'kv', scatter_dimension=1, tiled=True)  17.1 us
    all_gather x1, blocking collectives, local(): whole_rows = lax.all_gather(tokens, 'kv', axis=1, tiled=True)  15.4 us
    all_gather x1, blocking collectives, local(): hidden = lax.all_gather(own_hidden, 'kv', axis=1, tiled=True)  13.2 us
    reduce_sum x1, other arithmetic, local(): jnp.sum(state_next * out_map[:, :, None, :], axis=-1)  11.1 us
    dot_general x1, matrix products, local(): partial_mlp = jnp.dot(squared, w_down, preferred_element_type=jnp.float32)  8.84 us
    dot_general x1, matrix products, local(): jnp.dot(normed, w_maps, preferred_element_type=jnp.float32)  8.19 us
    dot_general x1, matrix products, local(): jnp.dot(heads_out, w_out, preferred_element_type=jnp.float32)  3.55 us
  transfers between devices with their start and end apart: 2, of which 2 were waited for; matrix products, arithmetic and copies ran while one was open for 1% of the time, Pallas kernels for 0%

commit v1 on v0

--- a/solution.py
+++ b/solution.py
@@ -1,13 +1,586 @@
+import functools
+
 import jax
 import jax.numpy as jnp
 from jax import lax
+from jax.experimental import pallas as pl
+from jax.experimental.pallas import tpu as pltpu
 from jax.sharding import PartitionSpec as P
 
 HEAD_DIM = 64
 STATE = 128
+MESH = pl.DeviceIdType.MESH
+VMEM_LIMIT = 60 * 1024 * 1024
 
 
 NORM_EPS = 1e-05
+NT = (((1,), (1,)), ((), ()))
+
+
+def greet(peers, me):
+    barrier = pltpu.get_barrier_semaphore()
+    for d in range(1, peers):
+        pl.semaphore_signal(
+            barrier, inc=1, device_id={"kv": lax.rem(me + d, peers)}, device_id_type=MESH
+        )
+    pl.semaphore_wait(barrier, peers - 1)
+
+
+def push(src, dst, send_sem, recv_sem, target):
+    return pltpu.make_async_remote_copy(
+        src_ref=src,
+        dst_ref=dst,
+        send_sem=send_sem,
+        recv_sem=recv_sem,
+        device_id={"kv": target},
+        device_id_type=MESH,
+    )
+
+
+def project_kernel(
+    peers,
+    tokens,
+    gain,
+    w_step,
+    bias,
+    decay_log,
+    w_gate,
+    w_value,
+    w_maps,
+    gate_out,
+    value_out,
+    maps_out,
+    step_out,
+    decay_out,
+    slots,
+    weights,
+    acc,
+    w_sem,
+    send_sem,
+    recv_sem,
+):
+    me = lax.axis_index("kv")
+    rows, part = tokens.shape
+    chunks, width = weights.shape[1], weights.shape[3]
+    heads = decay_out.shape[1]
+    inner = value_out.shape[1]
+
+    def source(c):
+        for ref in (w_gate, w_value, w_maps):
+            n = ref.shape[1] // width
+            if c < n:
+                return ref, c * width
+            c -= n
+
+    for d in range(peers):
+        start = pl.multiple_of(lax.rem(me + d, peers) * part, part)
+        for c in range(chunks):
+            ref, col = source(c)
+            pltpu.make_async_copy(
+                ref.at[pl.ds(start, part), pl.ds(col, width)], weights.at[d, c], w_sem.at[d, c]
+            ).start()
+
+    greet(peers, me)
+    sends = []
+    for d in range(1, peers):
+        cp = push(
+            tokens,
+            slots.at[peers - d],
+            send_sem.at[d],
+            recv_sem.at[peers - d],
+            lax.rem(me + d, peers),
+        )
+        cp.start()
+        sends.append(cp)
+
+    squares = jnp.zeros((rows, 1), jnp.float32)
+    step_pre = jnp.zeros((rows, w_step.shape[0]), jnp.float32)
+    for d in range(peers):
+        start = pl.multiple_of(lax.rem(me + d, peers) * part, part)
+        if d == 0:
+            raw = tokens[...]
+        else:
+            push(tokens, slots.at[d], send_sem.at[d], recv_sem.at[d], me).wait_recv()
+            raw = slots[d]
+        wide = raw.astype(jnp.float32)
+        squares = squares + jnp.sum(wide * wide, axis=1, keepdims=True)
+        scaled = (wide * gain[:, pl.ds(start, part)]).astype(jnp.bfloat16)
+        step_pre = step_pre + lax.dot_general(
+            scaled, w_step[:, pl.ds(start, part)], NT, preferred_element_type=jnp.float32
+        )
+
+        def chunk(c, carry, d=d, scaled=scaled):
+            pltpu.make_async_copy(
+                w_gate.at[pl.ds(0, part), pl.ds(0, width)], weights.at[d, c], w_sem.at[d, c]
+            ).wait()
+            out = jnp.dot(scaled, weights[d, c], preferred_element_type=jnp.float32)
+            acc[c] = out if d == 0 else acc[c] + out
+            return carry
+
+        lax.fori_loop(0, chunks, chunk, 0)
+
+    inv = lax.rsqrt(squares / (peers * part) + NORM_EPS)
+    for c in range(chunks):
+        total = acc[c] * inv
+        ref, col = source(c)
+        if ref is w_gate:
+            gate_out[:, pl.ds(col, width)] = total
+        elif ref is w_value:
+            value_out[:, pl.ds(col, width)] = total.astype(jnp.bfloat16)
+        else:
+            maps_out[:, pl.ds(col, width)] = total.astype(jnp.bfloat16)
+    step_pre = step_pre * inv
+    own = step_pre[:, :heads]
+    for j in range(1, peers):
+        own = jnp.where(me == j, step_pre[:, j * heads : (j + 1) * heads], own)
+    own = own + bias[...]
+    step = jnp.maximum(own, 0.0) + jnp.log1p(jnp.exp(-jnp.abs(own)))
+    decay_out[...] = jnp.exp(-step * jnp.exp(decay_log[...]))
+    lane = lax.broadcasted_iota(jnp.int32, (rows, 2 * HEAD_DIM), 1)
+    for h in range(0, heads, 2):
+        step_out[:, h * HEAD_DIM : (h + 2) * HEAD_DIM] = jnp.where(
+            lane < HEAD_DIM, step[:, h : h + 1], step[:, h + 1 : h + 2]
+        )
+    for cp in sends:
+        cp.wait_send()
+
+
+def project(peers, tokens, mix_gain, w_step, step_bias, decay_log, w_gate, w_value, w_maps):
+    rows, part = tokens.shape
+    heads = step_bias.shape[0]
+    inner, maps = w_value.shape[1], w_maps.shape[1]
+    width = min(1024, inner)
+    chunks = (2 * inner + maps) // width
+    f32 = jnp.float32
+    vmem = pl.BlockSpec(memory_space=pltpu.VMEM)
+    hbm = pl.BlockSpec(memory_space=pl.ANY)
+    return pl.pallas_call(
+        functools.partial(project_kernel, peers),
+        out_shape=(
+            jax.ShapeDtypeStruct((rows, inner), f32),
+            jax.ShapeDtypeStruct((rows, inner), jnp.bfloat16),
+            jax.ShapeDtypeStruct((rows, maps), jnp.bfloat16),
+            jax.ShapeDtypeStruct((rows, inner), f32),
+            jax.ShapeDtypeStruct((rows, heads), f32),
+        ),
+        in_specs=[vmem] * 5 + [hbm] * 3,
+        out_specs=(vmem,) * 5,
+        scratch_shapes=[
+            pltpu.VMEM((peers, rows, part), jnp.bfloat16),
+            pltpu.VMEM((peers, chunks, part, width), jnp.bfloat16),
+            pltpu.VMEM((chunks, rows, width), f32),
+            pltpu.SemaphoreType.DMA((peers, chunks)),
+            pltpu.SemaphoreType.DMA((peers,)),
+            pltpu.SemaphoreType.DMA((peers,)),
+        ],
+        compiler_params=pltpu.CompilerParams(
+            collective_id=0, has_side_effects=True, vmem_limit_bytes=VMEM_LIMIT
+        ),
+        name="project",
+    )(
+        tokens,
+        mix_gain[None, :],
+        w_step.T,
+        step_bias[None, :],
+        decay_log[None, :],
+        w_gate,
+        w_value,
+        w_maps,
+    )
+
+
+def silu(x):
+    return x * jax.nn.sigmoid(x)
+
+
+def state_kernel(
+    decay,
+    skip,
+    state,
+    gate,
+    value_new,
+    maps_new,
+    step,
+    past_value,
+    past_maps,
+    conv_value,
+    conv_maps,
+    head_gain,
+    heads_out,
+    state_out,
+    value_tail,
+    maps_tail,
+):
+    i = pl.program_id(0)
+    rows = state.shape[0]
+
+    def conv(past, new, taps, tail):
+        taps_n = past.shape[0]
+        total = new[...].astype(jnp.float32) * taps[taps_n : taps_n + 1, :]
+        for k in range(taps_n):
+            row = past[k]
+            total = total + row.astype(jnp.float32) * taps[k : k + 1, :]
+            if k > 0:
+                tail[k - 1] = row
+        tail[taps_n - 1] = new[...]
+        return silu(total)
+
+    value_act = conv(past_value, value_new, conv_value, value_tail)
+    maps_act = conv(past_maps, maps_new, conv_maps, maps_tail)
+    maps_act = maps_act.astype(jnp.bfloat16).astype(jnp.float32)
+
+    scaled = value_act * step[...]
+    high = scaled.astype(jnp.bfloat16).astype(jnp.float32)
+    both = jnp.concatenate([high, scaled - high], axis=0).T.astype(jnp.bfloat16)
+    ins = []
+    outs = []
+    for hh in range(2):
+        at = 2 * hh * STATE
+        ins.append(jnp.concatenate([maps_act[:, at : at + STATE]] * 2, axis=0))
+        outs.append(maps_act[:, at + STATE : at + 2 * STATE])
+    readers = jnp.concatenate(outs, axis=0).astype(jnp.bfloat16)
+
+    row = lax.broadcasted_iota(jnp.int32, (2 * rows, STATE), 0)
+    lane = lax.broadcasted_iota(jnp.int32, (2 * rows, STATE), 1)
+    seq = jnp.where(row >= rows, row - rows, row)
+    owner = jnp.where((row >= rows) == (lane >= HEAD_DIM), seq, -1)
+    read = jnp.zeros((2 * rows, 2 * HEAD_DIM), jnp.float32)
+    for b in range(0, rows, 2):
+        fresh = [None] * 4
+        for hh in range(2):
+            spread = jnp.concatenate(
+                [jnp.where(seq == b + k, ins[hh], 0.0) for k in range(2)], axis=1
+            ).astype(jnp.bfloat16)
+            written = jnp.dot(
+                both[hh * HEAD_DIM : (hh + 1) * HEAD_DIM],
+                spread,
+                preferred_element_type=jnp.float32,
+            )
+            for k in range(2):
+                new = (
+                    decay[b + k, 2 * i + hh] * state[b + k, hh]
+                    + written[:, k * STATE : (k + 1) * STATE]
+                )
+                state_out[b + k, hh] = new
+                fresh[2 * k + hh] = new.astype(jnp.bfloat16)
+        found = lax.dot_general(
+            readers, jnp.concatenate(fresh, axis=0), NT, preferred_element_type=jnp.float32
+        )
+        for k in range(2):
+            read = read + jnp.where(
+                owner == b + k, found[:, k * 2 * HEAD_DIM : (k + 1) * 2 * HEAD_DIM], 0.0
+            )
+    first = lane[:rows] < HEAD_DIM
+    read_out = read[:rows] + read[rows:]
+    read_out = read_out + jnp.where(first, skip[2 * i], skip[2 * i + 1]) * value_act
+    gated = read_out * silu(gate[...])
+    square = gated * gated
+    low = jnp.sum(jnp.where(first, square, 0.0), axis=1, keepdims=True)
+    top = jnp.sum(jnp.where(first, 0.0, square), axis=1, keepdims=True)
+    inv = lax.rsqrt(jnp.where(first, low, top) / HEAD_DIM + NORM_EPS)
+    heads_out[...] = (gated * inv * head_gain[...]).astype(jnp.bfloat16)
+
+
+def step_state(
+    decay,
+    skip_gain,
+    state,
+    gate,
+    value_new,
+    maps_new,
+    step,
+    past_value,
+    past_maps,
+    conv_value,
+    conv_maps,
+    head_gain,
+):
+    rows, heads = state.shape[:2]
+    smem = pl.BlockSpec(memory_space=pltpu.SMEM)
+    pair = 2 * HEAD_DIM
+    wide = 4 * STATE
+    taps = conv_value.shape[0]
+    past_v = jnp.swapaxes(past_value, 0, 1)
+    past_m = jnp.swapaxes(past_maps, 0, 1)
+    flat = lambda width: pl.BlockSpec((rows, width), lambda i: (0, i))
+    conv_spec = lambda width: pl.BlockSpec((taps, width), lambda i: (0, i))
+    past_spec = lambda width: pl.BlockSpec((taps - 1, rows, width), lambda i: (0, 0, i))
+    state_spec = pl.BlockSpec((rows, 2, HEAD_DIM, STATE), lambda i: (0, i, 0, 0))
+    heads_out, state_next, tail_v, tail_m = pl.pallas_call(
+        state_kernel,
+        grid=(heads // 2,),
+        out_shape=(
+            jax.ShapeDtypeStruct((rows, heads * HEAD_DIM), jnp.bfloat16),
+            jax.ShapeDtypeStruct(state.shape, jnp.float32),
+            jax.ShapeDtypeStruct(past_v.shape, jnp.bfloat16),
+            jax.ShapeDtypeStruct(past_m.shape, jnp.bfloat16),
+        ),
+        in_specs=[
+            smem,
+            smem,
+            state_spec,
+            flat(pair),
+            flat(pair),
+            flat(wide),
+            flat(pair),
+            past_spec(pair),
+            past_spec(wide),
+            conv_spec(pair),
+            conv_spec(wide),
+            pl.BlockSpec((1, pair), lambda i: (0, i)),
+        ],
+        out_specs=(flat(pair), state_spec, past_spec(pair), past_spec(wide)),
+        compiler_params=pltpu.CompilerParams(
+            dimension_semantics=("arbitrary",), vmem_limit_bytes=VMEM_LIMIT
+        ),
+        name="step_state",
+    )(
+        decay,
+        skip_gain,
+        state,
+        gate,
+        value_new,
+        maps_new,
+        step,
+        past_v,
+        past_m,
+        conv_value,
+        conv_maps,
+        head_gain[None, :],
+    )
+    return heads_out, state_next, jnp.swapaxes(tail_v, 0, 1), jnp.swapaxes(tail_m, 0, 1)
+
+
+def mixer_kernel(
+    peers,
+    heads,
+    tokens,
+    gain,
+    w_out,
+    w_up,
+    w_down,
+    layer_out,
+    out_w,
+    up_w,
+    down_w,
+    sums_a,
+    land_a,
+    own_hidden,
+    hidden,
+    up_acc,
+    squared,
+    sums_b,
+    land_b,
+    out_sem,
+    up_sem,
+    down_sem,
+    send_a,
+    recv_a,
+    send_h,
+    recv_h,
+    send_b,
+    recv_b,
+):
+    me = lax.axis_index("kv")
+    rows, part = tokens.shape
+    n_up, width = up_w.shape[1], up_w.shape[3]
+
+    def place(d):
+        return pl.multiple_of(lax.rem(me + d, peers) * part, part)
+
+    order = list(range(1, peers)) + [0]
+    waits_out, waits_down = {}, {}
+    for d in order:
+        cp = pltpu.make_async_copy(w_out.at[:, pl.ds(place(d), part)], out_w.at[d], out_sem.at[d])
+        cp.start()
+        waits_out[d] = cp
+    for d in range(peers):
+        for c in range(n_up):
+            pltpu.make_async_copy(
+                w_up.at[pl.ds(place(d), part), pl.ds(c * width, width)],
+                up_w.at[d, c],
+                up_sem.at[d, c],
+            ).start()
+    for d in order:
+        cp = pltpu.make_async_copy(
+            w_down.at[:, pl.ds(place(d), part)], down_w.at[d], down_sem.at[d]
+        )
+        cp.start()
+        waits_down[d] = cp
+
+    greet(peers, me)
+    pending = []
+
+    def scatter(left, weights, waits, sums, land, send, recv):
+        for d in order:
+            waits[d].wait()
+            piece = jnp.dot(left, weights[d], preferred_element_type=jnp.float32)
+            if d == 0:
+                total = piece
+            else:
+                sums[d] = piece
+                cp = push(
+                    sums.at[d],
+                    land.at[peers - d],
+                    send.at[d],
+                    recv.at[peers - d],
+                    lax.rem(me + d, peers),
+                )
+                cp.start()
+                pending.append(cp)
+        for d in range(1, peers):
+            push(sums.at[d], land.at[d], send.at[d], recv.at[d], me).wait_recv()
+            total = total + land[d]
+        return total
+
+    total = scatter(heads[...], out_w, waits_out, sums_a, land_a, send_a, recv_a)
+    mine = (tokens[...].astype(jnp.float32) + total).astype(jnp.bfloat16)
+    own_hidden[...] = mine
+    for d in range(1, peers):
+        cp = push(
+            own_hidden,
+            hidden.at[peers - d],
+            send_h.at[d],
+            recv_h.at[peers - d],
+            lax.rem(me + d, peers),
+        )
+        cp.start()
+        pending.append(cp)
+
+    squares = jnp.zeros((rows, 1), jnp.float32)
+    for d in range(peers):
+        if d == 0:
+            raw = mine
+        else:
+            push(own_hidden, hidden.at[d], send_h.at[d], recv_h.at[d], me).wait_recv()
+            raw = hidden[d]
+        wide = raw.astype(jnp.float32)
+        squares = squares + jnp.sum(wide * wide, axis=1, keepdims=True)
+        scaled = (wide * gain[:, pl.ds(place(d), part)]).astype(jnp.bfloat16)
+
+        def chunk(c, carry, d=d, scaled=scaled):
+            pltpu.make_async_copy(
+                w_up.at[pl.ds(0, part), pl.ds(0, width)], up_w.at[d, c], up_sem.at[d, c]
+            ).wait()
+            out = jnp.dot(scaled, up_w[d, c], preferred_element_type=jnp.float32)
+            up_acc[c] = out if d == 0 else up_acc[c] + out
+            return carry
+
+        lax.fori_loop(0, n_up, chunk, 0)
+
+    inv = lax.rsqrt(squares / (peers * part) + NORM_EPS)
+    for c in range(n_up):
+        up = jnp.maximum(up_acc[c] * inv, 0.0)
+        squared[:, c * width : (c + 1) * width] = (up * up).astype(jnp.bfloat16)
+    total = scatter(squared[...], down_w, waits_down, sums_b, land_b, send_b, recv_b)
+    layer_out[...] = (mine.astype(jnp.float32) + total).astype(jnp.bfloat16)
+    for cp in pending:
+        cp.wait_send()
+
+
+def mix_channels(peers, heads_out, tokens, mlp_gain, w_out, w_up, w_down):
+    rows, part = tokens.shape
+    inner, hid = w_out.shape[0], w_up.shape[1]
+    width = min(1024, hid)
+    f32, bf16 = jnp.float32, jnp.bfloat16
+    vmem = pl.BlockSpec(memory_space=pltpu.VMEM)
+    hbm = pl.BlockSpec(memory_space=pl.ANY)
+    sems = pltpu.SemaphoreType.DMA((peers,))
+    return pl.pallas_call(
+        functools.partial(mixer_kernel, peers),
+        out_shape=jax.ShapeDtypeStruct((rows, part), bf16),
+        in_specs=[vmem] * 3 + [hbm] * 3,
+        out_specs=vmem,
+        scratch_shapes=[
+            pltpu.VMEM((peers, inner, part), bf16),
+            pltpu.VMEM((peers, hid // width, part, width), bf16),
+            pltpu.VMEM((peers, hid, part), bf16),
+            pltpu.VMEM((peers, rows, part), f32),
+            pltpu.VMEM((peers, rows, part), f32),
+            pltpu.VMEM((rows, part), bf16),
+            pltpu.VMEM((peers, rows, part), bf16),
+            pltpu.VMEM((hid // width, rows, width), f32),
+            pltpu.VMEM((rows, hid), bf16),
+            pltpu.VMEM((peers, rows, part), f32),
+            pltpu.VMEM((peers, rows, part), f32),
+            sems,
+            pltpu.SemaphoreType.DMA((peers, hid // width)),
+            sems,
+            sems,
+            sems,
+            sems,
+            sems,
+            sems,
+            sems,
+        ],
+        compiler_params=pltpu.CompilerParams(
+            collective_id=1, has_side_effects=True, vmem_limit_bytes=VMEM_LIMIT
+        ),
+        name="mix_channels",
+    )(heads_out, tokens, mlp_gain[None, :], w_out, w_up, w_down)
+
+
+def local_kernels(
+    peers,
+    tokens,
+    mix_gain,
+    w_gate,
+    w_value,
+    w_maps,
+    w_step,
+    conv_value,
+    conv_maps,
+    past_value,
+    past_maps,
+    step_bias,
+    decay_log,
+    skip_gain,
+    head_gain,
+    state,
+    w_out,
+    mlp_gain,
+    w_up,
+    w_down,
+):
+    gate, value_new, maps_new, step, decay = project(
+        peers, tokens, mix_gain, w_step, step_bias, decay_log, w_gate, w_value, w_maps
+    )
+    heads_out, state_next, value_tail, maps_tail = step_state(
+        decay,
+        skip_gain,
+        state,
+        gate,
+        value_new,
+        maps_new,
+        step,
+        past_value,
+        past_maps,
+        conv_value,
+        conv_maps,
+        head_gain,
+    )
+    layer_out = mix_channels(peers, heads_out, tokens, mlp_gain, w_out, w_up, w_down)
+    return layer_out, state_next, value_tail, maps_tail
+
+
+def kernels_fit(peers, tokens, state, w_maps, w_up):
+    rows, part = tokens.shape
+    heads = state.shape[1]
+    inner = heads * HEAD_DIM
+    width = min(1024, inner)
+    held = 2 * tokens.shape[1] * peers * (2 * inner + w_maps.shape[1])
+    return (
+        peers > 1
+        and rows % 8 == 0
+        and part % 128 == 0
+        and heads % 2 == 0
+        and w_maps.shape[1] == heads * 2 * STATE
+        and inner % width == 0
+        and width % 128 == 0
+        and w_up.shape[1] % min(1024, w_up.shape[1]) == 0
+        and w_up.shape[1] % 128 == 0
+        and held <= 32 * 1024 * 1024
+    )
 
 
 def rms_rows(matrix, gain_vec):
@@ -116,4 +689,13 @@
         P(("dp", "tp"), None, "kv"),
         P(("dp", "tp"), None, "kv"),
     )
-    return jax.shard_map(local, mesh=mesh, in_specs=in_specs, out_specs=out_specs, check_vma=False)
+    peers = mesh.shape["kv"]
+
+    def device_part(*args):
+        if kernels_fit(peers, args[0], args[14], args[4], args[17]):
+            return local_kernels(peers, *args)
+        return local(*args)
+
+    return jax.shard_map(
+        device_part, mesh=mesh, in_specs=in_specs, out_specs=out_specs, check_vma=False
+    )

time: 127 us -> 56.2 us (0.44)
  Pallas kernels: 0 us -> 53.8 us
  waiting for transfers between devices: 37.3 us -> 0 us
  blocking collectives: 28.6 us -> 0 us
  matrix products: 27.3 us -> 0 us
  other arithmetic: 16.7 us -> 0 us
  between operations: 14.2 us -> 0.65 us
    pallas_call x0 -> x3, Pallas kernels: none -> 53.8 us  [the longest x1 22.8 us: mix_channels(): pl.pallas_call(functools.partial(mixer_kernel, peers), out_shape=jax.Shap...]
    reduce_scatter x2 -> x0, waiting for transfers between devices: 37.2 us -> none  [the longest x1 20.1 us: local(): lax.psum_scatter(partial_value, 'kv', scatter_dimension=1, tiled=True)]
    all_gather x2 -> x0, blocking collectives: 28.6 us -> none  [the longest x1 15.4 us: local(): whole_rows = lax.all_gather(tokens, 'kv', axis=1, tiled=True)]
    dot_general x6 -> x0, matrix products: 27.3 us -> none  [the longest x1 8.84 us: local(): partial_mlp = jnp.dot(squared, w_down, preferred_element_type=jnp.float32)]
    reduce_sum x6 -> x0, other arithmetic: 12.7 us -> none  [the longest x1 11.1 us: local(): jnp.sum(state_next * out_map[:, :, None, :], axis=-1)]
    convert_element_type x3 -> x0, other arithmetic: 2.33 us -> none  [the longest x1 1.41 us: local(): layer_out = (own_hidden.astype(jnp.float32) + mlp_part).astype(jnp.bfloat16)]
    concatenate x2 -> x0, other arithmetic: 1.54 us -> none  [short_conv(): window = jnp.concatenate([past_rows, newest[:, None, :]], axis=1)]
    unnamed x20 -> x1, local copies, waits for them, and re-layouts: 0.06 us -> 1.35 us
  transfers between devices with their start and end apart: 2 -> 0, of which waited for: 2 -> 0; matrix products, arithmetic and copies ran while one was open for 1% -> 0% of each run, Pallas kernels for 0% -> 0%
where the time goes in v1:
time: 56.2 us; the launch traced here: 55.8 us
  Pallas kernels  53.8 us (96%)
  local copies, waits for them, and re-layouts  1.35 us (2%)
  between operations  0.65 us (1%)
    pallas_call x1, Pallas kernels, mix_channels(): pl.pallas_call(functools.partial(mixer_kernel, peers), out_shape=jax.Shap...  22.8 us
    pallas_call x1, Pallas kernels, project(): pl.pallas_call(functools.partial(project_kernel, peers), out_shape=(jax.S...  15.9 us
    pallas_call x1, Pallas kernels, step_state(): pl.pallas_call(state_kernel, grid=(heads // 2,), out_shape=(jax.ShapeDtyp...  15.1 us
    unnamed x1, local copies, waits for them, and re-layouts  1.35 us

profile of v1, /device:TPU:0, one launch (start us, length us, event | category | flops | bytes accessed | tf_op | source)
XLA Modules:
  0.0 55.8 jit_solution(4740263704490026998)
XLA Ops:
  0.6 15.9 %project.1 = (f32[24,1024]{1,0:T(8,128)}, bf16[24,1024]{1,0:T(8,128)(2,1)}, bf16[24,4096]{1,0:T(8,128)(2,1)}, f32[24,1024]{1,0:T(8,128)}, f32[24,16]{1,0:T(8,128)}) custom-call(bf16[24,512]{1,0:T(8,128)(2,1)} %tokens.3, f32[1,2048]{1,0:T(1,128)} %bitcast.13, bf16[64,2048]{1,0:T(8,128)(2,1)} %bitcast.11, f32[1,16]{1,0:T(1,128)} %bitcast.16, ...), custom_call_target="tpu_custom_call" | custom-call | tf_op jit(solution)/shard_map/project/pallas_call | solution.py:157
  16.5 15.1 %step_state.1 = (bf16[24,1024]{1,0:T(8,128)(2,1)}, f32[24,16,64,128]{3,2,1,0:T(8,128)}, bf16[3,24,1024]{2,1,0:T(8,128)(2,1)}, bf16[3,24,4096]{2,1,0:T(8,128)(2,1)}) custom-call(f32[24,16]{1,0:T(8,128)} %get-tuple-element.13.decay, f32[16]{0:T(128)} %skip.1, f32[24,16,64,128]{3,2,1,0:T(8,128)} %state.1, f32[24,1024]{1,0:T(8,128)} %get-tuple-element.14.gate, ...), custom_call_target="tpu_custom_call" | custom-call | tf_op jit(solution)/shard_map/step_state/pallas_call | solution.py:309
  31.6 22.8 %mix_channels.1 = bf16[24,512]{1,0:T(8,128)(2,1)} custom-call(bf16[24,1024]{1,0:T(8,128)(2,1)} %get-tuple-element.18.heads, bf16[24,512]{1,0:T(8,128)(2,1)} %tokens.3, f32[1,2048]{1,0:T(1,128)} %bitcast.14, bf16[1024,2048]{1,0:T(8,128)(2,1)} %w_out.1, bf16[2048,2048]{1,0:T(8,128)(2,1)} %w_up.1, bf16[2048,2048]{1,0:T(8,128)(2,1)} %w_down.1), custom_call_target="tpu_custom_call" | custom-call | tf_op jit(solution)/shard_map/mix_channels/pallas_call | solution.py:489
  54.5 1.3 %copy.24 = bf16[24,512]{1,0:T(8,128)(2,1)} copy(bf16[24,512]{1,0:T(8,128)(2,1)} %mix_channels.1) | data formatting | bytes 49152

commit v2 on v1

--- a/solution.py
+++ b/solution.py
@@ -18,12 +18,21 @@
 
 
 def greet(peers, me):
-    barrier = pltpu.get_barrier_semaphore()
     for d in range(1, peers):
         pl.semaphore_signal(
-            barrier, inc=1, device_id={"kv": lax.rem(me + d, peers)}, device_id_type=MESH
+            pltpu.get_barrier_semaphore(),
+            inc=1,
+            device_id={"kv": lax.rem(me + d, peers)},
+            device_id_type=MESH,
         )
-    pl.semaphore_wait(barrier, peers - 1)
+
+
+def all_here(peers):
+    pl.semaphore_wait(pltpu.get_barrier_semaphore(), peers - 1)
+
+
+def far_first(peers):
+    return sorted(range(1, peers), key=lambda d: -min(d, peers - d))
 
 
 def push(src, dst, send_sem, recv_sem, target):
@@ -46,43 +55,36 @@
     decay_log,
     w_gate,
     w_value,
-    w_maps,
+    normed_out,
     gate_out,
     value_out,
-    maps_out,
     step_out,
     decay_out,
     slots,
     weights,
-    acc,
     w_sem,
     send_sem,
     recv_sem,
 ):
     me = lax.axis_index("kv")
     rows, part = tokens.shape
-    chunks, width = weights.shape[1], weights.shape[3]
+    chunks, width = weights.shape[0], weights.shape[2]
     heads = decay_out.shape[1]
-    inner = value_out.shape[1]
-
-    def source(c):
-        for ref in (w_gate, w_value, w_maps):
-            n = ref.shape[1] // width
-            if c < n:
-                return ref, c * width
-            c -= n
-
-    for d in range(peers):
-        start = pl.multiple_of(lax.rem(me + d, peers) * part, part)
-        for c in range(chunks):
-            ref, col = source(c)
-            pltpu.make_async_copy(
-                ref.at[pl.ds(start, part), pl.ds(col, width)], weights.at[d, c], w_sem.at[d, c]
-            ).start()
+    half = chunks // 2
 
     greet(peers, me)
+    loads = []
+    for c in range(chunks):
+        ref = w_gate if c < half else w_value
+        cp = pltpu.make_async_copy(
+            ref.at[:, pl.ds((c % half) * width, width)], weights.at[c], w_sem.at[c]
+        )
+        cp.start()
+        loads.append(cp)
+
+    all_here(peers)
     sends = []
-    for d in range(1, peers):
+    for d in far_first(peers):
         cp = push(
             tokens,
             slots.at[peers - d],
@@ -93,43 +95,33 @@
         cp.start()
         sends.append(cp)
 
+    def place(d):
+        return pl.multiple_of(lax.rem(me + d, peers) * part, part)
+
     squares = jnp.zeros((rows, 1), jnp.float32)
-    step_pre = jnp.zeros((rows, w_step.shape[0]), jnp.float32)
-    for d in range(peers):
-        start = pl.multiple_of(lax.rem(me + d, peers) * part, part)
-        if d == 0:
-            raw = tokens[...]
+    raws = []
+    for d in [0] + far_first(peers)[::-1]:
+        if d > 0:
+            push(tokens, slots.at[d], send_sem.at[d], recv_sem.at[d], me).wait_recv()
+        raw = (tokens[...] if d == 0 else slots[d]).astype(jnp.float32)
+        squares = squares + jnp.sum(raw * raw, axis=1, keepdims=True)
+        raws.append((d, raw))
+    inv = lax.rsqrt(squares / (peers * part) + NORM_EPS)
+    for d, raw in raws:
+        normed_out[:, pl.ds(place(d), part)] = (
+            raw * inv * gain[:, pl.ds(place(d), part)]
+        ).astype(jnp.bfloat16)
+
+    normed = normed_out[...]
+    step_pre = lax.dot_general(normed, w_step[...], NT, preferred_element_type=jnp.float32)
+    for c in range(chunks):
+        loads[c].wait()
+        out = jnp.dot(normed, weights[c], preferred_element_type=jnp.float32)
+        at = pl.ds((c % half) * width, width)
+        if c < half:
+            gate_out[:, at] = out
         else:
-            push(tokens, slots.at[d], send_sem.at[d], recv_sem.at[d], me).wait_recv()
-            raw = slots[d]
-        wide = raw.astype(jnp.float32)
-        squares = squares + jnp.sum(wide * wide, axis=1, keepdims=True)
-        scaled = (wide * gain[:, pl.ds(start, part)]).astype(jnp.bfloat16)
-        step_pre = step_pre + lax.dot_general(
-            scaled, w_step[:, pl.ds(start, part)], NT, preferred_element_type=jnp.float32
-        )
-
-        def chunk(c, carry, d=d, scaled=scaled):
-            pltpu.make_async_copy(
-                w_gate.at[pl.ds(0, part), pl.ds(0, width)], weights.at[d, c], w_sem.at[d, c]
-            ).wait()
-            out = jnp.dot(scaled, weights[d, c], preferred_element_type=jnp.float32)
-            acc[c] = out if d == 0 else acc[c] + out
-            return carry
-
-        lax.fori_loop(0, chunks, chunk, 0)
-
-    inv = lax.rsqrt(squares / (peers * part) + NORM_EPS)
-    for c in range(chunks):
-        total = acc[c] * inv
-        ref, col = source(c)
-        if ref is w_gate:
-            gate_out[:, pl.ds(col, width)] = total
-        elif ref is w_value:
-            value_out[:, pl.ds(col, width)] = total.astype(jnp.bfloat16)
-        else:
-            maps_out[:, pl.ds(col, width)] = total.astype(jnp.bfloat16)
-    step_pre = step_pre * inv
+            value_out[:, at] = out.astype(jnp.bfloat16)
     own = step_pre[:, :heads]
     for j in range(1, peers):
         own = jnp.where(me == j, step_pre[:, j * heads : (j + 1) * heads], own)
@@ -145,31 +137,30 @@
         cp.wait_send()
 
 
-def project(peers, tokens, mix_gain, w_step, step_bias, decay_log, w_gate, w_value, w_maps):
+def project(peers, tokens, mix_gain, w_step, step_bias, decay_log, w_gate, w_value):
     rows, part = tokens.shape
     heads = step_bias.shape[0]
-    inner, maps = w_value.shape[1], w_maps.shape[1]
-    width = min(1024, inner)
-    chunks = (2 * inner + maps) // width
-    f32 = jnp.float32
+    model, inner = w_value.shape
+    width = min(512, inner)
+    chunks = 2 * inner // width
+    f32, bf16 = jnp.float32, jnp.bfloat16
     vmem = pl.BlockSpec(memory_space=pltpu.VMEM)
     hbm = pl.BlockSpec(memory_space=pl.ANY)
     return pl.pallas_call(
         functools.partial(project_kernel, peers),
         out_shape=(
+            jax.ShapeDtypeStruct((rows, model), bf16),
             jax.ShapeDtypeStruct((rows, inner), f32),
-            jax.ShapeDtypeStruct((rows, inner), jnp.bfloat16),
-            jax.ShapeDtypeStruct((rows, maps), jnp.bfloat16),
+            jax.ShapeDtypeStruct((rows, inner), bf16),
             jax.ShapeDtypeStruct((rows, inner), f32),
             jax.ShapeDtypeStruct((rows, heads), f32),
         ),
-        in_specs=[vmem] * 5 + [hbm] * 3,
+        in_specs=[vmem] * 5 + [hbm] * 2,
         out_specs=(vmem,) * 5,
         scratch_shapes=[
-            pltpu.VMEM((peers, rows, part), jnp.bfloat16),
-            pltpu.VMEM((peers, chunks, part, width), jnp.bfloat16),
-            pltpu.VMEM((chunks, rows, width), f32),
-            pltpu.SemaphoreType.DMA((peers, chunks)),
+            pltpu.VMEM((peers, rows, part), bf16),
+            pltpu.VMEM((chunks, model, width), bf16),
+            pltpu.SemaphoreType.DMA((chunks,)),
             pltpu.SemaphoreType.DMA((peers,)),
             pltpu.SemaphoreType.DMA((peers,)),
         ],
@@ -185,7 +176,6 @@
         decay_log[None, :],
         w_gate,
         w_value,
-        w_maps,
     )
 
 
@@ -199,7 +189,8 @@
     state,
     gate,
     value_new,
-    maps_new,
+    normed,
+    w_maps,
     step,
     past_value,
     past_maps,
@@ -216,16 +207,18 @@
 
     def conv(past, new, taps, tail):
         taps_n = past.shape[0]
-        total = new[...].astype(jnp.float32) * taps[taps_n : taps_n + 1, :]
+        total = new.astype(jnp.float32) * taps[taps_n : taps_n + 1, :]
         for k in range(taps_n):
             row = past[k]
             total = total + row.astype(jnp.float32) * taps[k : k + 1, :]
             if k > 0:
                 tail[k - 1] = row
-        tail[taps_n - 1] = new[...]
+        tail[taps_n - 1] = new
         return silu(total)
 
-    value_act = conv(past_value, value_new, conv_value, value_tail)
+    maps_new = jnp.dot(normed[...], w_maps[...], preferred_element_type=jnp.float32)
+    maps_new = maps_new.astype(jnp.bfloat16)
+    value_act = conv(past_value, value_new[...], conv_value, value_tail)
     maps_act = conv(past_maps, maps_new, conv_maps, maps_tail)
     maps_act = maps_act.astype(jnp.bfloat16).astype(jnp.float32)
 
@@ -287,7 +280,8 @@
     state,
     gate,
     value_new,
-    maps_new,
+    normed,
+    w_maps,
     step,
     past_value,
     past_maps,
@@ -321,7 +315,8 @@
             state_spec,
             flat(pair),
             flat(pair),
-            flat(wide),
+            pl.BlockSpec(normed.shape, lambda i: (0, 0)),
+            pl.BlockSpec((w_maps.shape[0], wide), lambda i: (0, i)),
             flat(pair),
             past_spec(pair),
             past_spec(wide),
@@ -340,7 +335,8 @@
         state,
         gate,
         value_new,
-        maps_new,
+        normed,
+        w_maps,
         step,
         past_v,
         past_m,
@@ -388,7 +384,8 @@
     def place(d):
         return pl.multiple_of(lax.rem(me + d, peers) * part, part)
 
-    order = list(range(1, peers)) + [0]
+    order = far_first(peers) + [0]
+    greet(peers, me)
     waits_out, waits_down = {}, {}
     for d in order:
         cp = pltpu.make_async_copy(w_out.at[:, pl.ds(place(d), part)], out_w.at[d], out_sem.at[d])
@@ -408,7 +405,6 @@
         cp.start()
         waits_down[d] = cp
 
-    greet(peers, me)
     pending = []
 
     def scatter(left, weights, waits, sums, land, send, recv):
@@ -418,7 +414,9 @@
             if d == 0:
                 total = piece
             else:
-                sums[d] = piece
+                sums[d] = piece.astype(jnp.bfloat16)
+                if not pending:
+                    all_here(peers)
                 cp = push(
                     sums.at[d],
                     land.at[peers - d],
@@ -430,7 +428,7 @@
                 pending.append(cp)
         for d in range(1, peers):
             push(sums.at[d], land.at[d], send.at[d], recv.at[d], me).wait_recv()
-            total = total + land[d]
+            total = total + land[d].astype(jnp.float32)
         return total
 
     total = scatter(heads[...], out_w, waits_out, sums_a, land_a, send_a, recv_a)
@@ -456,13 +454,16 @@
             raw = hidden[d]
         wide = raw.astype(jnp.float32)
         squares = squares + jnp.sum(wide * wide, axis=1, keepdims=True)
-        scaled = (wide * gain[:, pl.ds(place(d), part)]).astype(jnp.bfloat16)
+        scaled = wide * gain[:, pl.ds(place(d), part)]
+        high = scaled.astype(jnp.bfloat16).astype(jnp.float32)
+        scaled = jnp.concatenate([high, scaled - high], axis=0).astype(jnp.bfloat16)
 
         def chunk(c, carry, d=d, scaled=scaled):
             pltpu.make_async_copy(
                 w_up.at[pl.ds(0, part), pl.ds(0, width)], up_w.at[d, c], up_sem.at[d, c]
             ).wait()
             out = jnp.dot(scaled, up_w[d, c], preferred_element_type=jnp.float32)
+            out = out[:rows] + out[rows:]
             up_acc[c] = out if d == 0 else up_acc[c] + out
             return carry
 
@@ -481,7 +482,7 @@
 def mix_channels(peers, heads_out, tokens, mlp_gain, w_out, w_up, w_down):
     rows, part = tokens.shape
     inner, hid = w_out.shape[0], w_up.shape[1]
-    width = min(1024, hid)
+    width = min(2048, hid)
     f32, bf16 = jnp.float32, jnp.bfloat16
     vmem = pl.BlockSpec(memory_space=pltpu.VMEM)
     hbm = pl.BlockSpec(memory_space=pl.ANY)
@@ -495,14 +496,14 @@
             pltpu.VMEM((peers, inner, part), bf16),
             pltpu.VMEM((peers, hid // width, part, width), bf16),
             pltpu.VMEM((peers, hid, part), bf16),
-            pltpu.VMEM((peers, rows, part), f32),
-            pltpu.VMEM((peers, rows, part), f32),
+            pltpu.VMEM((peers, rows, part), bf16),
+            pltpu.VMEM((peers, rows, part), bf16),
             pltpu.VMEM((rows, part), bf16),
             pltpu.VMEM((peers, rows, part), bf16),
             pltpu.VMEM((hid // width, rows, width), f32),
             pltpu.VMEM((rows, hid), bf16),
-            pltpu.VMEM((peers, rows, part), f32),
-            pltpu.VMEM((peers, rows, part), f32),
+            pltpu.VMEM((peers, rows, part), bf16),
+            pltpu.VMEM((peers, rows, part), bf16),
             sems,
             pltpu.SemaphoreType.DMA((peers, hid // width)),
             sems,
@@ -542,8 +543,8 @@
     w_up,
     w_down,
 ):
-    gate, value_new, maps_new, step, decay = project(
-        peers, tokens, mix_gain, w_step, step_bias, decay_log, w_gate, w_value, w_maps
+    normed, gate, value_new, step, decay = project(
+        peers, tokens, mix_gain, w_step, step_bias, decay_log, w_gate, w_value
     )
     heads_out, state_next, value_tail, maps_tail = step_state(
         decay,
@@ -551,7 +552,8 @@
         state,
         gate,
         value_new,
-        maps_new,
+        normed,
+        w_maps,
         step,
         past_value,
         past_maps,
@@ -567,7 +569,7 @@
     rows, part = tokens.shape
     heads = state.shape[1]
     inner = heads * HEAD_DIM
-    width = min(1024, inner)
+    width = min(512, inner)
     held = 2 * tokens.shape[1] * peers * (2 * inner + w_maps.shape[1])
     return (
         peers > 1
@@ -577,7 +579,7 @@
         and w_maps.shape[1] == heads * 2 * STATE
         and inner % width == 0
         and width % 128 == 0
-        and w_up.shape[1] % min(1024, w_up.shape[1]) == 0
+        and w_up.shape[1] % min(2048, w_up.shape[1]) == 0
         and w_up.shape[1] % 128 == 0
         and held <= 32 * 1024 * 1024
     )

time: 56.2 us -> 55 us (0.979)
  Pallas kernels: 53.8 us -> 52.8 us
    pallas_call x1, Pallas kernels: 15.1 us -> 19.7 us  [step_state(): pl.pallas_call(state_kernel, grid=(heads // 2,), out_shape=(jax.ShapeDtyp...]
    pallas_call x1, Pallas kernels: 15.9 us -> 12.2 us  [project(): pl.pallas_call(functools.partial(project_kernel, peers), out_shape=(jax.S...]
    pallas_call x1, Pallas kernels: 22.8 us -> 20.9 us  [mix_channels(): pl.pallas_call(functools.partial(mixer_kernel, peers), out_shape=jax.Shap...]
where the time goes in v2:
time: 55 us; the launch traced here: 54.8 us
  Pallas kernels  52.8 us (96%)
  local copies, waits for them, and re-layouts  1.35 us (2%)
  between operations  0.65 us (1%)
    pallas_call x1, Pallas kernels, mix_channels(): pl.pallas_call(functools.partial(mixer_kernel, peers), out_shape=jax.Shap...  20.9 us
    pallas_call x1, Pallas kernels, step_state(): pl.pallas_call(state_kernel, grid=(heads // 2,), out_shape=(jax.ShapeDtyp...  19.7 us
    pallas_call x1, Pallas kernels, project(): pl.pallas_call(functools.partial(project_kernel, peers), out_shape=(jax.S...  12.2 us
    unnamed x1, local copies, waits for them, and re-layouts  1.35 us

profile of v2, /device:TPU:0, one launch (start us, length us, event | category | flops | bytes accessed | tf_op | source)
XLA Modules:
  0.0 54.8 jit_solution(13154145177180458437)
XLA Ops:
  0.6 12.2 %project.1 = (bf16[24,2048]{1,0:T(8,128)(2,1)}, f32[24,1024]{1,0:T(8,128)}, bf16[24,1024]{1,0:T(8,128)(2,1)}, f32[24,1024]{1,0:T(8,128)}, f32[24,16]{1,0:T(8,128)}) custom-call(bf16[24,512]{1,0:T(8,128)(2,1)} %tokens.3, f32[1,2048]{1,0:T(1,128)} %bitcast.13, bf16[64,2048]{1,0:T(8,128)(2,1)} %bitcast.11, f32[1,16]{1,0:T(1,128)} %bitcast.16, ...), custom_call_target="tpu_custom_call" | custom-call | tf_op jit(solution)/shard_map/project/pallas_call | solution.py:149
  12.8 19.7 %step_state.1 = (bf16[24,1024]{1,0:T(8,128)(2,1)}, f32[24,16,64,128]{3,2,1,0:T(8,128)}, bf16[3,24,1024]{2,1,0:T(8,128)(2,1)}, bf16[3,24,4096]{2,1,0:T(8,128)(2,1)}) custom-call(f32[24,16]{1,0:T(8,128)} %get-tuple-element.13.decay, f32[16]{0:T(128)} %skip.1, f32[24,16,64,128]{3,2,1,0:T(8,128)} %state.1, f32[24,1024]{1,0:T(8,128)} %get-tuple-element.14.gate, ...), custom_call_target="tpu_custom_call" | custom-call | tf_op jit(solution)/shard_map/step_state/pallas_call | solution.py:303
  32.6 20.9 %mix_channels.1 = bf16[24,512]{1,0:T(8,128)(2,1)} custom-call(bf16[24,1024]{1,0:T(8,128)(2,1)} %get-tuple-element.18.heads, bf16[24,512]{1,0:T(8,128)(2,1)} %tokens.3, f32[1,2048]{1,0:T(1,128)} %bitcast.14, bf16[1024,2048]{1,0:T(8,128)(2,1)} %w_out.1, bf16[2048,2048]{1,0:T(8,128)(2,1)} %w_up.1, bf16[2048,2048]{1,0:T(8,128)(2,1)} %w_down.1), custom_call_target="tpu_custom_call" | custom-call | tf_op jit(solution)/shard_map/mix_channels/pallas_call | solution.py:490
  53.4 1.3 %copy.24 = bf16[24,512]{1,0:T(8,128)(2,1)} copy(bf16[24,512]{1,0:T(8,128)(2,1)} %mix_channels.1) | data formatting | bytes 49152

commit v3 on v1

--- a/solution.py
+++ b/solution.py
@@ -18,12 +18,21 @@
 
 
 def greet(peers, me):
-    barrier = pltpu.get_barrier_semaphore()
     for d in range(1, peers):
         pl.semaphore_signal(
-            barrier, inc=1, device_id={"kv": lax.rem(me + d, peers)}, device_id_type=MESH
+            pltpu.get_barrier_semaphore(),
+            inc=1,
+            device_id={"kv": lax.rem(me + d, peers)},
+            device_id_type=MESH,
         )
-    pl.semaphore_wait(barrier, peers - 1)
+
+
+def all_here(peers):
+    pl.semaphore_wait(pltpu.get_barrier_semaphore(), peers - 1)
+
+
+def far_first(peers):
+    return sorted(range(1, peers), key=lambda d: -min(d, peers - d))
 
 
 def push(src, dst, send_sem, recv_sem, target):
@@ -64,25 +73,26 @@
     chunks, width = weights.shape[1], weights.shape[3]
     heads = decay_out.shape[1]
     inner = value_out.shape[1]
-
-    def source(c):
-        for ref in (w_gate, w_value, w_maps):
-            n = ref.shape[1] // width
-            if c < n:
-                return ref, c * width
-            c -= n
-
-    for d in range(peers):
+    greet(peers, me)
+
+    for d in [0] + far_first(peers)[::-1]:
         start = pl.multiple_of(lax.rem(me + d, peers) * part, part)
-        for c in range(chunks):
-            ref, col = source(c)
+        for k, ref in enumerate((w_gate, w_value)):
             pltpu.make_async_copy(
-                ref.at[pl.ds(start, part), pl.ds(col, width)], weights.at[d, c], w_sem.at[d, c]
+                ref.at[pl.ds(start, part), :],
+                weights.at[d, 0, :, pl.ds(k * inner, inner)],
+                w_sem.at[d, 0],
             ).start()
-
-    greet(peers, me)
+        for c in range(1, chunks):
+            pltpu.make_async_copy(
+                w_maps.at[pl.ds(start, part), pl.ds((c - 1) * width, width)],
+                weights.at[d, c],
+                w_sem.at[d, c],
+            ).start()
+
+    all_here(peers)
     sends = []
-    for d in range(1, peers):
+    for d in far_first(peers):
         cp = push(
             tokens,
             slots.at[peers - d],
@@ -94,8 +104,8 @@
         sends.append(cp)
 
     squares = jnp.zeros((rows, 1), jnp.float32)
-    step_pre = jnp.zeros((rows, w_step.shape[0]), jnp.float32)
-    for d in range(peers):
+    step_pre = jnp.zeros((2 * rows, w_step.shape[0]), jnp.float32)
+    for d in [0] + far_first(peers)[::-1]:
         start = pl.multiple_of(lax.rem(me + d, peers) * part, part)
         if d == 0:
             raw = tokens[...]
@@ -104,32 +114,30 @@
             raw = slots[d]
         wide = raw.astype(jnp.float32)
         squares = squares + jnp.sum(wide * wide, axis=1, keepdims=True)
-        scaled = (wide * gain[:, pl.ds(start, part)]).astype(jnp.bfloat16)
+        scaled = wide * gain[:, pl.ds(start, part)]
+        high = scaled.astype(jnp.bfloat16).astype(jnp.float32)
+        scaled = jnp.concatenate([high, scaled - high], axis=0).astype(jnp.bfloat16)
         step_pre = step_pre + lax.dot_general(
             scaled, w_step[:, pl.ds(start, part)], NT, preferred_element_type=jnp.float32
         )
 
-        def chunk(c, carry, d=d, scaled=scaled):
+        for c in range(chunks):
             pltpu.make_async_copy(
-                w_gate.at[pl.ds(0, part), pl.ds(0, width)], weights.at[d, c], w_sem.at[d, c]
+                w_maps.at[pl.ds(0, part), pl.ds(0, width)], weights.at[d, c], w_sem.at[d, c]
             ).wait()
             out = jnp.dot(scaled, weights[d, c], preferred_element_type=jnp.float32)
+            out = out[:rows] + out[rows:]
             acc[c] = out if d == 0 else acc[c] + out
-            return carry
-
-        lax.fori_loop(0, chunks, chunk, 0)
 
     inv = lax.rsqrt(squares / (peers * part) + NORM_EPS)
     for c in range(chunks):
         total = acc[c] * inv
-        ref, col = source(c)
-        if ref is w_gate:
-            gate_out[:, pl.ds(col, width)] = total
-        elif ref is w_value:
-            value_out[:, pl.ds(col, width)] = total.astype(jnp.bfloat16)
+        if c == 0:
+            gate_out[...] = total[:, :inner]
+            value_out[...] = total[:, inner:].astype(jnp.bfloat16)
         else:
-            maps_out[:, pl.ds(col, width)] = total.astype(jnp.bfloat16)
-    step_pre = step_pre * inv
+            maps_out[:, (c - 1) * width : c * width] = total.astype(jnp.bfloat16)
+    step_pre = (step_pre[:rows] + step_pre[rows:]) * inv
     own = step_pre[:, :heads]
     for j in range(1, peers):
         own = jnp.where(me == j, step_pre[:, j * heads : (j + 1) * heads], own)
@@ -149,8 +157,8 @@
     rows, part = tokens.shape
     heads = step_bias.shape[0]
     inner, maps = w_value.shape[1], w_maps.shape[1]
-    width = min(1024, inner)
-    chunks = (2 * inner + maps) // width
+    width = 2 * inner
+    chunks = 1 + maps // width
     f32 = jnp.float32
     vmem = pl.BlockSpec(memory_space=pltpu.VMEM)
     hbm = pl.BlockSpec(memory_space=pl.ANY)
@@ -388,7 +396,8 @@
     def place(d):
         return pl.multiple_of(lax.rem(me + d, peers) * part, part)
 
-    order = list(range(1, peers)) + [0]
+    order = far_first(peers) + [0]
+    greet(peers, me)
     waits_out, waits_down = {}, {}
     for d in order:
         cp = pltpu.make_async_copy(w_out.at[:, pl.ds(place(d), part)], out_w.at[d], out_sem.at[d])
@@ -408,7 +417,6 @@
         cp.start()
         waits_down[d] = cp
 
-    greet(peers, me)
     pending = []
 
     def scatter(left, weights, waits, sums, land, send, recv):
@@ -418,7 +426,9 @@
             if d == 0:
                 total = piece
             else:
-                sums[d] = piece
+                sums[d] = piece.astype(jnp.bfloat16)
+                if not pending:
+                    all_here(peers)
                 cp = push(
                     sums.at[d],
                     land.at[peers - d],
@@ -430,7 +440,7 @@
                 pending.append(cp)
         for d in range(1, peers):
             push(sums.at[d], land.at[d], send.at[d], recv.at[d], me).wait_recv()
-            total = total + land[d]
+            total = total + land[d].astype(jnp.float32)
         return total
 
     total = scatter(heads[...], out_w, waits_out, sums_a, land_a, send_a, recv_a)
@@ -456,13 +466,16 @@
             raw = hidden[d]
         wide = raw.astype(jnp.float32)
         squares = squares + jnp.sum(wide * wide, axis=1, keepdims=True)
-        scaled = (wide * gain[:, pl.ds(place(d), part)]).astype(jnp.bfloat16)
+        scaled = wide * gain[:, pl.ds(place(d), part)]
+        high = scaled.astype(jnp.bfloat16).astype(jnp.float32)
+        scaled = jnp.concatenate([high, scaled - high], axis=0).astype(jnp.bfloat16)
 
         def chunk(c, carry, d=d, scaled=scaled):
             pltpu.make_async_copy(
                 w_up.at[pl.ds(0, part), pl.ds(0, width)], up_w.at[d, c], up_sem.at[d, c]
             ).wait()
             out = jnp.dot(scaled, up_w[d, c], preferred_element_type=jnp.float32)
+            out = out[:rows] + out[rows:]
             up_acc[c] = out if d == 0 else up_acc[c] + out
             return carry
 
@@ -481,7 +494,7 @@
 def mix_channels(peers, heads_out, tokens, mlp_gain, w_out, w_up, w_down):
     rows, part = tokens.shape
     inner, hid = w_out.shape[0], w_up.shape[1]
-    width = min(1024, hid)
+    width = min(2048, hid)
     f32, bf16 = jnp.float32, jnp.bfloat16
     vmem = pl.BlockSpec(memory_space=pltpu.VMEM)
     hbm = pl.BlockSpec(memory_space=pl.ANY)
@@ -495,14 +508,14 @@
             pltpu.VMEM((peers, inner, part), bf16),
             pltpu.VMEM((peers, hid // width, part, width), bf16),
             pltpu.VMEM((peers, hid, part), bf16),
-            pltpu.VMEM((peers, rows, part), f32),
-            pltpu.VMEM((peers, rows, part), f32),
+            pltpu.VMEM((peers, rows, part), bf16),
+            pltpu.VMEM((peers, rows, part), bf16),
             pltpu.VMEM((rows, part), bf16),
             pltpu.VMEM((peers, rows, part), bf16),
             pltpu.VMEM((hid // width, rows, width), f32),
             pltpu.VMEM((rows, hid), bf16),
-            pltpu.VMEM((peers, rows, part), f32),
-            pltpu.VMEM((peers, rows, part), f32),
+            pltpu.VMEM((peers, rows, part), bf16),
+            pltpu.VMEM((peers, rows, part), bf16),
             sems,
             pltpu.SemaphoreType.DMA((peers, hid // width)),
             sems,
@@ -577,7 +590,7 @@
         and w_maps.shape[1] == heads * 2 * STATE
         and inner % width == 0
         and width % 128 == 0
-        and w_up.shape[1] % min(1024, w_up.shape[1]) == 0
+        and w_up.shape[1] % min(2048, w_up.shape[1]) == 0
         and w_up.shape[1] % 128 == 0
         and held <= 32 * 1024 * 1024
     )

time: 56.2 us -> 52.6 us (0.936)
  Pallas kernels: 53.8 us -> 50.3 us
    pallas_call x1, Pallas kernels: 22.8 us -> 20.9 us  [mix_channels(): pl.pallas_call(functools.partial(mixer_kernel, peers), out_shape=jax.Shap...]
    pallas_call x1, Pallas kernels: 15.9 us -> 14.3 us  [project(): pl.pallas_call(functools.partial(project_kernel, peers), out_shape=(jax.S...]
where the time goes in v3:
time: 52.6 us; the launch traced here: 52.3 us
  Pallas kernels  50.3 us (96%)
  local copies, waits for them, and re-layouts  1.35 us (3%)
  between operations  0.65 us (1%)
    pallas_call x1, Pallas kernels, mix_channels(): pl.pallas_call(functools.partial(mixer_kernel, peers), out_shape=jax.Shap...  20.9 us
    pallas_call x1, Pallas kernels, step_state(): pl.pallas_call(state_kernel, grid=(heads // 2,), out_shape=(jax.ShapeDtyp...  15.2 us
    pallas_call x1, Pallas kernels, project(): pl.pallas_call(functools.partial(project_kernel, peers), out_shape=(jax.S...  14.3 us
    unnamed x1, local copies, waits for them, and re-layouts  1.35 us

profile of v3, /device:TPU:0, one launch (start us, length us, event | category | flops | bytes accessed | tf_op | source)
XLA Modules:
  0.0 52.3 jit_solution(6606926298884658887)
XLA Ops:
  0.6 14.3 %project.1 = (f32[24,1024]{1,0:T(8,128)}, bf16[24,1024]{1,0:T(8,128)(2,1)}, bf16[24,4096]{1,0:T(8,128)(2,1)}, f32[24,1024]{1,0:T(8,128)}, f32[24,16]{1,0:T(8,128)}) custom-call(bf16[24,512]{1,0:T(8,128)(2,1)} %tokens.3, f32[1,2048]{1,0:T(1,128)} %bitcast.13, bf16[64,2048]{1,0:T(8,128)(2,1)} %bitcast.11, f32[1,16]{1,0:T(1,128)} %bitcast.16, ...), custom_call_target="tpu_custom_call" | custom-call | tf_op jit(solution)/shard_map/project/pallas_call | solution.py:165
  14.9 15.2 %step_state.1 = (bf16[24,1024]{1,0:T(8,128)(2,1)}, f32[24,16,64,128]{3,2,1,0:T(8,128)}, bf16[3,24,1024]{2,1,0:T(8,128)(2,1)}, bf16[3,24,4096]{2,1,0:T(8,128)(2,1)}) custom-call(f32[24,16]{1,0:T(8,128)} %get-tuple-element.13.decay, f32[16]{0:T(128)} %skip.1, f32[24,16,64,128]{3,2,1,0:T(8,128)} %state.1, f32[24,1024]{1,0:T(8,128)} %get-tuple-element.14.gate, ...), custom_call_target="tpu_custom_call" | custom-call | tf_op jit(solution)/shard_map/step_state/pallas_call | solution.py:317
  30.1 20.9 %mix_channels.1 = bf16[24,512]{1,0:T(8,128)(2,1)} custom-call(bf16[24,1024]{1,0:T(8,128)(2,1)} %get-tuple-element.18.heads, bf16[24,512]{1,0:T(8,128)(2,1)} %tokens.3, f32[1,2048]{1,0:T(1,128)} %bitcast.14, bf16[1024,2048]{1,0:T(8,128)(2,1)} %w_out.1, bf16[2048,2048]{1,0:T(8,128)(2,1)} %w_up.1, bf16[2048,2048]{1,0:T(8,128)(2,1)} %w_down.1), custom_call_target="tpu_custom_call" | custom-call | tf_op jit(solution)/shard_map/mix_channels/pallas_call | solution.py:502
  50.9 1.3 %copy.24 = bf16[24,512]{1,0:T(8,128)(2,1)} copy(bf16[24,512]{1,0:T(8,128)(2,1)} %mix_channels.1) | data formatting | bytes 49152
